TPU v7x, 32 devices: a whole 2x2x4 slice. The times are simulated.
32 devices in a mesh: fs: 8 (over z, y), tp: 4 (over x, core).
Axes of the slice: x: 2, y: 2, z: 4, core: 2. Of those that a mesh axis runs over, the one named last changes fastest.
Arguments:
- tokens: bfloat16 [8192, 2048], P('fs', 'tp'), may hold values from -6 to 6
- mix_gain: float32 [2048], replicated, may hold values from 0.1 to 1.9
- in_weight: float32 [2048, 1024], P('fs', 'tp'), may hold values from -0.125 to 0.125
- in_scale: float32 [1024], P('tp'), may hold values from 0.4 to 2.5
- out_weight: float32 [1024, 2048], P('tp', 'fs'), may hold values from -0.1875 to 0.1875
- out_scale: float32 [2048], P('fs'), may hold values from 0.4 to 2.5
- ffn_gain: float32 [2048], replicated, may hold values from 0.1 to 1.9
- gate_weight: float32 [2048, 6144], P('fs', 'tp'), may hold values from -0.125 to 0.125
- gate_scale: float32 [6144], P('tp'), may hold values from 0.4 to 2.5
- up_weight: float32 [2048, 6144], P('fs', 'tp'), may hold values from -0.125 to 0.125
- up_scale: float32 [6144], P('tp'), may hold values from 0.4 to 2.5
- down_weight: float32 [6144, 2048], P('tp', 'fs'), may hold values from -0.078125 to 0.078125
- down_scale: float32 [2048], P('fs'), may hold values from 0.4 to 2.5
Outputs:
- layer_out: bfloat16 [8192, 2048], P('fs', 'tp')
All inputs are finite; a program needn't handle non-finite values.
Results may differ from a plain program's by a relative error of at most 0.023.
Values may be sent and summed in bfloat16 or wider, within the bound.
A program may use at most 128 MiB of HBM per device.

v0:
```python
import jax
import jax.numpy as jnp
from jax import lax
from jax.sharding import PartitionSpec as P

D = 2048
GROUPS = 4
GRID_W = 64
GC = 256


WINDOWS = (2, 4, 8, 16)
EPSILON = 1e-06


def box_matrix(length, window):
    position = jnp.arange(length, dtype=jnp.int32)
    lower_end = jnp.clip(position - window // 2, 0, length)
    upper_end = jnp.clip(position + (window - window // 2), 0, length)
    inside = (position[None, :] >= lower_end[:, None]) & (position[None, :] < upper_end[:, None])
    return inside.astype(jnp.float32) / (upper_end - lower_end).astype(jnp.float32)[:, None]


def pooled_differences(channels, channel_offset):
    tokens_here, extent = channels.shape
    lattice = channels.reshape(tokens_here // GRID_W, GRID_W, extent)
    group_of = (channel_offset + jnp.arange(extent, dtype=jnp.int32)) // GC
    result = jnp.zeros_like(lattice)
    for group in range(GROUPS):
        window = WINDOWS[group]
        across = jnp.einsum(
            "jk,akc->ajc", box_matrix(GRID_W, window), lattice, precision=lax.Precision.HIGHEST
        )
        smoothed = jnp.einsum(
            "ab,bjc->ajc",
            box_matrix(lattice.shape[0], window),
            across,
            precision=lax.Precision.HIGHEST,
        )
        result = jnp.where((group_of == group)[None, None, :], smoothed, result)
    return (result - lattice).reshape(tokens_here, extent).astype(jnp.bfloat16)


def fold_rows(features, gain, weights):
    widened = lax.all_gather(features, "tp", axis=1, tiled=True).astype(jnp.float32)
    squares = jnp.sum(widened * widened, axis=1)
    scaled = (widened * gain).astype(jnp.bfloat16)
    totals = tuple(
        (jnp.dot(scaled, weight, preferred_element_type=jnp.float32) for weight in weights)
    )
    totals, squares = (totals, squares)
    inverse_rms = lax.rsqrt(squares / D + EPSILON)[:, None]
    return tuple((total * inverse_rms for total in totals))


def column_product(hidden, weight_columns, scales):
    partial_value = (
        jnp.dot(
            hidden,
            lax.all_gather(weight_columns, "fs", axis=1, tiled=True),
            preferred_element_type=jnp.float32,
        )
        * scales
    )
    return lax.psum_scatter(
        partial_value.astype(jnp.bfloat16), "tp", scatter_dimension=1, tiled=True
    ).astype(jnp.float32)


def local(
    tokens,
    mix_gain,
    in_weight,
    in_scale,
    out_weight,
    out_scale,
    ffn_gain,
    gate_weight,
    gate_scale,
    up_weight,
    up_scale,
    down_weight,
    down_scale,
):
    out_scales, down_scales = (
        lax.all_gather(out_scale, "fs", axis=0, tiled=True),
        lax.all_gather(down_scale, "fs", axis=0, tiled=True),
    )
    in_full, gate_full, up_full = (
        lax.all_gather(in_weight.astype(jnp.bfloat16), "fs", axis=0, tiled=True),
        lax.all_gather(gate_weight.astype(jnp.bfloat16), "fs", axis=0, tiled=True),
        lax.all_gather(up_weight.astype(jnp.bfloat16), "fs", axis=0, tiled=True),
    )
    (channels,) = fold_rows(tokens, mix_gain, (in_full,))
    channels = channels * in_scale
    pooled = pooled_differences(channels, lax.axis_index("tp") * channels.shape[1])
    mixed = column_product(pooled, out_weight.astype(jnp.bfloat16), out_scales)
    residual = (tokens.astype(jnp.float32) + mixed).astype(jnp.bfloat16)
    gate_value, up_value = fold_rows(residual, ffn_gain, (gate_full, up_full))
    gate_value = gate_value * gate_scale
    up_value = up_value * up_scale
    hidden = (jax.nn.silu(gate_value) * up_value).astype(jnp.bfloat16)
    channel_out = column_product(hidden, down_weight.astype(jnp.bfloat16), down_scales)
    return (residual.astype(jnp.float32) + channel_out).astype(jnp.bfloat16)


def solution(mesh):
    return jax.shard_map(
        local,
        mesh=mesh,
        in_specs=(
            P("fs", "tp"),
            P(),
            P("fs", "tp"),
            P("tp"),
            P("tp", "fs"),
            P("fs"),
            P(),
            P("fs", "tp"),
            P("tp"),
            P("fs", "tp"),
            P("tp"),
            P("tp", "fs"),
            P("fs"),
        ),
        out_specs=P("fs", "tp"),
        check_vma=False,
    )
```

profile of v0, /device:TPU:0, one launch (start us, length us, event | category | flops | bytes accessed | tf_op | source)
XLA Modules:
  0.0 587.0 jit_solution(10302616835622095069)
XLA Ops:
  6.5 0.0 all-gather.10.cloned.1.call-start
  6.5 0.7 all-gather.10.cloned.1.call-update
  7.3 0.0 all-gather.12.cloned.1.call-start
  7.3 1.6 convert_element_type.145
  8.9 0.0 all-gather.12.cloned.1.call-update
  9.0 0.0 all-gather.14.cloned.1.call-start
  9.0 1.6 convert_element_type.162
  10.6 0.0 all-gather.14.cloned.1.call-update
  10.6 0.0 reduce-scatter.3.cloned.1.call-start
  11.0 22.6 %all-gather = f32[8,1,256]{2,1,0:T(1,128)S(1)} all-gather(f32[1,1,256]{2,1,0:T(1,128)} %bitcast.61), channel_id=1, replica_groups=mesh['fs'=8,'tp'=4] {'fs'}, dimensions={0}, use_global_device_ids=true | all-gather | bytes 9216 | tf_op jit(solution)/shard_map/all_gather | solution.py:86
  33.5 12.6 %all-gather.10.cloned.1.call-done = bf16[1024,2048]{1,0:T(8,128)(2,1)} async-done(((bf16[1024,512]{1,0:T(8,128)(2,1)}), bf16[1024,2048]{1,0:T(8,128)(2,1)}) %all-gather.10.cloned.1.call-update) | async-done | bytes 4194320 | tf_op jit(solution)/shard_map/all_gather | solution.py:45
  46.1 3.1 fusion.1
  49.2 39.4 %all-gather.12.cloned.1.call-done = bf16[2048,256]{1,0:T(8,128)(2,1)} async-done(((bf16[256,256]{1,0:T(8,128)(2,1)}), bf16[2048,256]{1,0:T(8,128)(2,1)}) %all-gather.12.cloned.1.call-update) | async-done | bytes 1048592 | tf_op jit(solution)/shard_map/all_gather | solution.py:90
  88.5 0.0 copy-done.5
  88.5 0.0 copy-done.9
  88.5 3.7 fusion.14
  92.3 1.1 convolution_bitcast_fusion
  93.4 1.1 convolution_bitcast_fusion.1
  94.4 1.1 convolution_bitcast_fusion.2
  95.5 1.1 convolution_bitcast_fusion.3
  96.6 1.5 convolution_select_fusion
  98.1 1.5 convolution_select_fusion.1
  99.6 1.5 convolution_select_fusion.2
  101.1 2.3 fusion.17
  103.4 0.2 copy.22
  103.5 25.2 %all-gather.14.cloned.1.call-done = bf16[256,2048]{1,0:T(8,128)(2,1)} async-done(((bf16[256,256]{1,0:T(8,128)(2,1)}), bf16[256,2048]{1,0:T(8,128)(2,1)}) %all-gather.14.cloned.1.call-update) | async-done | bytes 1048592 | tf_op jit(solution)/shard_map/all_gather | solution.py:60
  128.7 4.5 multiply_convert_fusion.1
  133.3 0.0 reduce-scatter.3.cloned.1.call-update
  133.3 0.0 copy-start.4
  133.3 0.0 all-gather.16.cloned.1.call-start
  133.4 43.5 %reduce-scatter.3.cloned.1.call-done = bf16[1024,512]{1,0:T(8,128)(2,1)} async-done(((bf16[1024,2048]{1,0:T(8,128)(2,1)}), bf16[1024,512]{1,0:T(8,128)(2,1)}) %reduce-scatter.3.cloned.1.call-update) | async-done | bytes 1048592 | tf_op jit(solution)/shard_map/reduce_scatter | solution.py:65
  176.9 0.0 copy-done.1
  176.9 2.5 add_convert_fusion.1
  179.4 0.0 all-gather.16.cloned.1.call-update
  179.4 0.0 copy-start.6
  179.4 0.0 all-gather.18.cloned.1.call-start
  179.5 0.0 copy-done.2
  179.5 1.0 convert_element_type.169
  180.5 0.0 all-gather.18.cloned.1.call-update
  180.5 0.0 all-gather.20.cloned.1.call-start
  180.5 2.4 convert_element_type.170
  182.9 0.0 all-gather.20.cloned.1.call-update
  183.0 0.0 all-gather.22.cloned.1.call-start
  183.0 0.0 copy-done.3
  183.0 1.0 convert_element_type.172
  184.0 0.0 all-gather.22.cloned.1.call-update
  184.0 0.0 reduce-scatter.5.cloned.1.call-start
  184.1 0.0 copy-done.4
  184.1 20.5 %all-gather.1 = f32[8,1,256]{2,1,0:T(1,128)S(1)} all-gather(f32[1,1,256]{2,1,0:T(1,128)S(1)} %bitcast.62), channel_id=1, replica_groups=mesh['fs'=8,'tp'=4] {'fs'}, dimensions={0}, use_global_device_ids=true | all-gather | bytes 9216 | tf_op jit(solution)/shard_map/all_gather | solution.py:87
  204.6 9.4 %all-gather.16.cloned.1.call-done = bf16[1024,2048]{1,0:T(8,128)(2,1)} async-done(((bf16[1024,512]{1,0:T(8,128)(2,1)}), bf16[1024,2048]{1,0:T(8,128)(2,1)}) %all-gather.16.cloned.1.call-update) | async-done | bytes 4194320 | tf_op jit(solution)/shard_map/all_gather | solution.py:45
  214.0 3.1 fusion.3
  217.1 0.0 copy-start.7
  217.1 0.0 copy-start.8
  217.1 97.7 %all-gather.18.cloned.1.call-done = bf16[2048,1536]{1,0:T(8,128)(2,1)} async-done(((bf16[256,1536]{1,0:T(8,128)(2,1)}), bf16[2048,1536]{1,0:T(8,128)(2,1)}) %all-gather.18.cloned.1.call-update) | async-done | bytes 6291472 | tf_op jit(solution)/shard_map/all_gather | solution.py:91
  314.8 0.0 copy-done.6
  314.8 11.7 %fusion.8 = f32[1024,1536]{1,0:T(8,128)} fusion(bf16[2048,1536]{1,0:T(8,128)(2,1)} %all-gather.18.cloned.1.call-done, bf16[1024,2048]{1,0:T(8,128)(2,1)} %all-gather.16.cloned.1.call-done, f32[2048]{0:T(1024)S(1)} %copy-done.6), kind=kOutput, calls=%fused_computation.13 | convolution fusion | flops 6448742400 | bytes 16785408 | tf_op jit(solution)/shard_map/dot_general | solution.py:49
  326.5 87.4 %all-gather.20.cloned.1.call-done = bf16[2048,1536]{1,0:T(8,128)(2,1)} async-done(((bf16[256,1536]{1,0:T(8,128)(2,1)}), bf16[2048,1536]{1,0:T(8,128)(2,1)}) %all-gather.20.cloned.1.call-update) | async-done | bytes 6291472 | tf_op jit(solution)/shard_map/all_gather | solution.py:92
  413.8 99.7 %all-gather.22.cloned.1.call-done = bf16[1536,2048]{1,0:T(8,128)(2,1)} async-done(((bf16[1536,256]{1,0:T(8,128)(2,1)}), bf16[1536,2048]{1,0:T(8,128)(2,1)}) %all-gather.22.cloned.1.call-update) | async-done | bytes 6291472 | tf_op jit(solution)/shard_map/all_gather | solution.py:60
  513.6 0.0 copy-done.7
  513.6 0.0 copy-done.8
  513.6 21.6 %multiply_convert_fusion = bf16[1024,2048]{1,0:T(8,128)(2,1)} fusion(bf16[1536,2048]{1,0:T(8,128)(2,1)} %all-gather.22.cloned.1.call-done, f32[2048]{0:T(1024)S(1)} %bitcast.60, f32[1024,1536]{1,0:T(8,128)} %fusion.8, bf16[2048,1536]{1,0:T(8,128)(2,1)} %all-gather.20.cloned.1.call-done, bf16[1024,2048]{1,0:T(8,128)(2,1)} %all-gather.16.cloned.1.call-done, ...), kind=kOutput, calls=%fused_computation.8 | convolution fusion | flops 12911116288 | bytes 27295744 | tf_op jit(solution)/shard_map/dot_general | solution.py:58
  535.2 0.0 reduce-scatter.5.cloned.1.call-update
  535.2 42.8 %reduce-scatter.5.cloned.1.call-done = bf16[1024,512]{1,0:T(8,128)(2,1)} async-done(((bf16[1024,2048]{1,0:T(8,128)(2,1)}), bf16[1024,512]{1,0:T(8,128)(2,1)}) %reduce-scatter.5.cloned.1.call-update) | async-done | bytes 1048592 | tf_op jit(solution)/shard_map/reduce_scatter | solution.py:65
  578.0 2.5 add_convert_fusion
  (27 shorter events, 0.2 us)
Async XLA Ops:
  6.5 82.0 %copy-start.5 = (f32[2048]{0:T(1024)S(1)}, f32[2048]{0:T(1024)}, u32[]{:S(2)}) copy-start(f32[2048]{0:T(1024)} %param.14) | copy-start | bytes 24580
  6.5 82.0 %copy-start.9 = (f32[256]{0:T(256)S(1)}, f32[256]{0:T(256)}, u32[]{:S(2)}) copy-start(f32[256]{0:T(256)} %param.16) | copy-start | bytes 3076
  6.5 39.6 %all-gather.10.cloned.1.call-start = ((), (), s32[]{:S(2)}) async-start(), calls=%async_computation.2 | async-start | bytes 5242880 | tf_op jit(solution)/shard_map/all_gather | solution.py:45
  7.3 81.3 %all-gather.12.cloned.1.call-start = ((), (), s32[]{:S(2)}) async-start(), calls=%async_computation.3 | async-start | bytes 1179648 | tf_op jit(solution)/shard_map/all_gather | solution.py:90
  9.0 119.8 %all-gather.14.cloned.1.call-start = ((), (), s32[]{:S(2)}) async-start(), calls=%async_computation.4 | async-start | bytes 1179648 | tf_op jit(solution)/shard_map/all_gather | solution.py:60
  10.6 166.2 %reduce-scatter.3.cloned.1.call-start = ((), (), s32[]{:S(2)}) async-start(), calls=%async_computation.5 | async-start | bytes 5242880 | tf_op jit(solution)/shard_map/reduce_scatter | solution.py:65
  128.7 48.1 %copy-start.1 = (bf16[1024,512]{1,0:T(8,128)(2,1)S(1)}, bf16[1024,512]{1,0:T(8,128)(2,1)}, u32[]{:S(2)}) copy-start(bf16[1024,512]{1,0:T(8,128)(2,1)} %param.13) | copy-start | bytes 3145732
  133.3 46.2 %copy-start.2 = (f32[256,1536]{1,0:T(8,128)S(1)}, f32[256,1536]{1,0:T(8,128)}, u32[]{:S(2)}) copy-start(f32[256,1536]{1,0:T(8,128)} %param.20) | copy-start | bytes 4718596
  133.3 50.8 %copy-start.4 = (f32[256]{0:T(256)S(1)}, f32[256]{0:T(256)}, u32[]{:S(2)}) copy-start(f32[256]{0:T(256)} %param.25) | copy-start | bytes 3076
  133.3 80.7 %all-gather.16.cloned.1.call-start = ((), (), s32[]{:S(2)}) async-start(), calls=%async_computation.6 | async-start | bytes 5242880 | tf_op jit(solution)/shard_map/all_gather | solution.py:45
  179.4 3.6 copy-start.3
  179.4 135.4 %copy-start.6 = (f32[2048]{0:T(1024)S(1)}, f32[2048]{0:T(1024)}, u32[]{:S(2)}) copy-start(f32[2048]{0:T(1024)} %param.19) | copy-start | bytes 24580
  179.4 135.4 %all-gather.18.cloned.1.call-start = ((), (), s32[]{:S(2)}) async-start(), calls=%async_computation.7 | async-start | bytes 7077888 | tf_op jit(solution)/shard_map/all_gather | solution.py:91
  180.5 233.4 %all-gather.20.cloned.1.call-start = ((), (), s32[]{:S(2)}) async-start(), calls=%async_computation.8 | async-start | bytes 7077888 | tf_op jit(solution)/shard_map/all_gather | solution.py:92
  183.0 330.6 %all-gather.22.cloned.1.call-start = ((), (), s32[]{:S(2)}) async-start(), calls=%async_computation.9 | async-start | bytes 7077888 | tf_op jit(solution)/shard_map/all_gather | solution.py:60
  184.0 394.0 %reduce-scatter.5.cloned.1.call-start = ((), (), s32[]{:S(2)}) async-start(), calls=%async_computation.10 | async-start | bytes 5242880 | tf_op jit(solution)/shard_map/reduce_scatter | solution.py:65
  217.1 296.5 %copy-start.7 = (f32[1536]{0:T(1024)S(1)}, f32[1536]{0:T(1024)}, u32[]{:S(2)}) copy-start(f32[1536]{0:T(1024)} %param.23) | copy-start | bytes 18436
  217.1 296.5 %copy-start.8 = (f32[1536]{0:T(1024)S(1)}, f32[1536]{0:T(1024)}, u32[]{:S(2)}) copy-start(f32[1536]{0:T(1024)} %param.21) | copy-start | bytes 18436
  513.6 64.4 %copy-start = (bf16[1024,512]{1,0:T(8,128)(2,1)S(1)}, bf16[1024,512]{1,0:T(8,128)(2,1)}, u32[]{:S(2)}) copy-start(bf16[1024,512]{1,0:T(8,128)(2,1)} %add_convert_fusion.1) | copy-start | bytes 3145732
Sparse Core Ops, SparseCore 0:
  8.9 37.1 all-gather.9
  48.2 40.2 all-gather.11
  90.6 38.0 all-gather.13
  133.4 43.4 reduce-scatter.2
  179.5 34.4 all-gather.15
  216.0 98.6 all-gather.17
  316.9 96.8 all-gather.19
  415.9 97.6 all-gather.21
  535.3 42.5 reduce-scatter.4
where the time goes:
time: 587 us
  waiting for transfers between devices  458 us (78%)
  matrix products  52.6 us (9%)
  blocking collectives  43.1 us (7%)
  other arithmetic  18.9 us (3%)
  between operations  13.5 us (2%)
    all_gather x2, waiting for transfers between devices, column_product(): lax.all_gather(weight_columns, 'fs', axis=1, tiled=True)  125 us
    all_gather x1, waiting for transfers between devices, local(): lax.all_gather(gate_weight.astype(jnp.bfloat16), 'fs', axis=0, tiled=True)  97.7 us
    all_gather x1, waiting for transfers between devices, local(): lax.all_gather(up_weight.astype(jnp.bfloat16), 'fs', axis=0, tiled=True)  87.4 us
    reduce_scatter x2, waiting for transfers between devices, column_product(): lax.psum_scatter(partial_value.astype(jnp.bfloat16), 'tp', scatter_dimens...  86.3 us
    all_gather x1, waiting for transfers between devices, local(): lax.all_gather(in_weight.astype(jnp.bfloat16), 'fs', axis=0, tiled=True)  39.4 us
    dot_general x2, matrix products, column_product(): jnp.dot(hidden, lax.all_gather(weight_columns, 'fs', axis=1, tiled=True),...  26.1 us
    all_gather x1, blocking collectives, local(): lax.all_gather(out_scale, 'fs', axis=0, tiled=True)  22.6 us
    all_gather x2, waiting for transfers between devices, fold_rows(): lax.all_gather(features, 'tp', axis=1, tiled=True).astype(jnp.float32)  22 us
  transfers between devices with their start and end apart: 9, of which 9 were waited for; matrix products, arithmetic and copies ran while one was open for 7% of the time, Pallas kernels for 0%

commit v1 on v0

v1 whole, which is shorter than its diff:
```python
import jax
import jax.numpy as jnp
from jax import lax
from jax.sharding import PartitionSpec as P

GROUPS = 4
GRID_W = 64
GC = 256
WINDOWS = (2, 4, 8, 16)
EPSILON = 1e-06


def box_matrix(length, window):
    position = jnp.arange(length, dtype=jnp.int32)
    lower_end = jnp.clip(position - window // 2, 0, length)
    upper_end = jnp.clip(position + (window - window // 2), 0, length)
    inside = (position[None, :] >= lower_end[:, None]) & (position[None, :] < upper_end[:, None])
    return inside.astype(jnp.float32) / (upper_end - lower_end).astype(jnp.float32)[:, None]


def smooth(lattice, window):
    across = jnp.einsum(
        "jk,akc->ajc", box_matrix(GRID_W, window), lattice, precision=lax.Precision.HIGHEST
    )
    return jnp.einsum(
        "ab,bjc->ajc",
        box_matrix(lattice.shape[0], window),
        across,
        precision=lax.Precision.HIGHEST,
    )


def pooled_differences(channels, channel_offset):
    tokens_here, extent = channels.shape
    lattice = channels.reshape(tokens_here // GRID_W, GRID_W, extent)
    if GC % extent == 0:
        result = smooth(lattice, jnp.asarray(WINDOWS, jnp.int32)[channel_offset // GC])
    else:
        group_of = (channel_offset + jnp.arange(extent, dtype=jnp.int32)) // GC
        result = jnp.zeros_like(lattice)
        for group in range(GROUPS):
            result = jnp.where(
                (group_of == group)[None, None, :], smooth(lattice, WINDOWS[group]), result
            )
    return (result - lattice).reshape(tokens_here, extent).astype(jnp.bfloat16)


class Grid:
    def __init__(self, fs, tp):
        self.ys = max(tp // 2, 1)
        self.zs = fs // self.ys
        index = lax.axis_index("fs")
        self.z, self.y = index // self.ys, index % self.ys

    def gather(self, block):
        rows = []
        for s in range(self.zs):
            pairs = [
                (z * self.ys + y, (z + s) % self.zs * self.ys + y)
                for z in range(self.zs)
                for y in range(self.ys)
            ]
            rows.append(lax.ppermute(block, "fs", pairs) if s else block)
        found = []
        for s, row in enumerate(rows):
            for t in range(self.ys):
                pairs = [
                    (z * self.ys + y, z * self.ys + (y + t) % self.ys)
                    for z in range(self.zs)
                    for y in range(self.ys)
                ]
                item = lax.ppermute(row, "fs", pairs) if t else row
                index = lax.rem(self.z - s + self.zs, self.zs) * self.ys + lax.rem(
                    self.y - t + self.ys, self.ys
                )
                found.append((index, item))
        return found


def stack(pieces):
    shape = (len(pieces),) + pieces[0][1].shape
    result = jnp.zeros(shape, pieces[0][1].dtype)
    for index, item in pieces:
        result = lax.dynamic_update_index_in_dim(result, item, index, 0)
    return result


def rows_of(pieces):
    whole = stack(pieces)
    return whole.reshape(whole.shape[0] * whole.shape[1], whole.shape[2])


def fold_rows(features, gain, weights):
    widened = lax.all_gather(features, "tp", axis=1, tiled=True)
    widened = widened.astype(jnp.float32)
    inverse_rms = lax.rsqrt(jnp.mean(widened * widened, axis=1) + EPSILON)[:, None]
    scaled = (widened * gain).astype(jnp.bfloat16)
    return tuple(
        jnp.dot(scaled, weight, preferred_element_type=jnp.float32) * inverse_rms
        for weight in weights
    )


def column_product(hidden, pieces):
    terms = stack(
        [
            (index, jnp.dot(hidden, item, preferred_element_type=jnp.float32).astype(jnp.bfloat16))
            for index, item in pieces
        ]
    )
    mine = lax.psum_scatter(terms, "tp", scatter_dimension=0, tiled=True)
    return mine.transpose(1, 0, 2).reshape(hidden.shape[0], -1).astype(jnp.float32)


def low(weight, scale=None):
    weight = weight.astype(jnp.bfloat16)
    if scale is None:
        return weight
    return (weight.astype(jnp.float32) * scale).astype(jnp.bfloat16)


def solution(mesh):
    fs, tp = mesh.shape["fs"], mesh.shape["tp"]

    def layer(
        tokens,
        mix_gain,
        in_weight,
        in_scale,
        out_weight,
        out_scale,
        ffn_gain,
        gate_weight,
        gate_scale,
        up_weight,
        up_scale,
        down_weight,
        down_scale,
    ):
        grid = Grid(fs, tp)
        wide = gate_weight.shape[1]
        both_pieces = grid.gather(jnp.concatenate([low(gate_weight), low(up_weight)], axis=1))
        down_pieces = grid.gather(low(down_weight, down_scale))
        small = lax.all_gather(
            jnp.stack([low(in_weight), low(out_weight, out_scale)]), "fs", axis=0
        )
        in_full = small[:, 0].reshape(-1, in_weight.shape[1])
        out_pieces = [(j, small[j, 1]) for j in range(fs)]
        (channels,) = fold_rows(tokens, mix_gain, (in_full,))
        channels = channels * in_scale
        pooled = pooled_differences(channels, lax.axis_index("tp") * channels.shape[1])
        mixed = column_product(pooled, out_pieces)
        residual = (tokens.astype(jnp.float32) + mixed).astype(jnp.bfloat16)
        (both,) = fold_rows(residual, ffn_gain, (rows_of(both_pieces),))
        gate_value = both[:, :wide] * gate_scale
        up_value = both[:, wide:] * up_scale
        hidden = (jax.nn.silu(gate_value) * up_value).astype(jnp.bfloat16)
        channel_out = column_product(hidden, down_pieces)
        return (residual.astype(jnp.float32) + channel_out).astype(jnp.bfloat16)

    return jax.shard_map(
        layer,
        mesh=mesh,
        in_specs=(
            P("fs", "tp"),
            P(),
            P("fs", "tp"),
            P("tp"),
            P("tp", "fs"),
            P("fs"),
            P(),
            P("fs", "tp"),
            P("tp"),
            P("fs", "tp"),
            P("tp"),
            P("tp", "fs"),
            P("fs"),
        ),
        out_specs=P("fs", "tp"),
        check_vma=False,
    )
```

time: 587 us -> 479 us (0.82)
  waiting for transfers between devices: 458 us -> 227 us
  starting transfers between devices: 0.34 us -> 101 us
  local copies, waits for them, and re-layouts: 0.21 us -> 56.4 us
  blocking collectives: 43.1 us -> 0 us
    all_gather x7 -> x3, waiting for transfers between devices: 371 us -> 80.9 us  [the longest x1 47.6 us: layer(): lax.all_gather(jnp.stack([low(in_weight), low(out_weight, out_scale)]), '...]
    ppermute x0 -> x14, starting transfers between devices: none -> 101 us  [the longest x6 91.6 us: gather(): rows.append(lax.ppermute(block, 'fs', pairs) if s else block)]
    ppermute x0 -> x14, waiting for transfers between devices: none -> 45.2 us  [the longest x6 45.2 us: gather(): rows.append(lax.ppermute(block, 'fs', pairs) if s else block)]
    all_gather x2 -> x0, blocking collectives: 43.1 us -> none  [the longest x1 22.6 us: local(): lax.all_gather(out_scale, 'fs', axis=0, tiled=True)]
    dynamic_update_slice x0 -> x16, local copies, waits for them, and re-layouts: none -> 23.5 us  [stack(): result = lax.dynamic_update_index_in_dim(result, item, index, 0)]
    broadcast_in_dim x0 -> x9, local copies, waits for them, and re-layouts: none -> 21.8 us  [the longest x8 15.7 us: stack(): result = lax.dynamic_update_index_in_dim(result, item, index, 0)]
    reduce_scatter x2, waiting for transfers between devices: 86.3 us -> 100 us  [column_product(): mine = lax.psum_scatter(terms, 'tp', scatter_dimension=0, tiled=True)]
    dot_general x12 -> x20, matrix products: 52.6 us -> 52.5 us  [the longest x16 31.2 us: column_product(): jnp.dot(hidden, item, preferred_element_type=jnp.float32)]
  transfers between devices with their start and end apart: 9 -> 19, of which waited for: 9 -> 7; matrix products, arithmetic and copies ran while one was open for 7% -> 20% of each run, Pallas kernels for 0% -> 0%
where the time goes in v1:
time: 479 us; the launch traced here: 478 us
  waiting for transfers between devices  227 us (47%)
  starting transfers between devices  101 us (21%)
  local copies, waits for them, and re-layouts  56.4 us (12%)
  matrix products  52.5 us (11%)
  other arithmetic  24.4 us (5%)
  between operations  16.7 us (3%)
    reduce_scatter x2, waiting for transfers between devices, column_product(): mine = lax.psum_scatter(terms, 'tp', scatter_dimension=0, tiled=True)  100 us
    ppermute x6, starting transfers between devices, gather(): rows.append(lax.ppermute(block, 'fs', pairs) if s else block)  91.6 us
    all_gather x1, waiting for transfers between devices, layer(): lax.all_gather(jnp.stack([low(in_weight), low(out_weight, out_scale)]), '...  47.6 us
    ppermute x6, waiting for transfers between devices, gather(): rows.append(lax.ppermute(block, 'fs', pairs) if s else block)  45.2 us
    all_gather x2, waiting for transfers between devices, fold_rows(): widened = lax.all_gather(features, 'tp', axis=1, tiled=True)  33.3 us
    dot_general x16, matrix products, column_product(): jnp.dot(hidden, item, preferred_element_type=jnp.float32)  31.2 us
    dynamic_update_slice x16, local copies, waits for them, and re-layouts, stack(): result = lax.dynamic_update_index_in_dim(result, item, index, 0)  23.5 us
    dot_general x2, matrix products, fold_rows(): jnp.dot(scaled, weight, preferred_element_type=jnp.float32) * inverse_rms  18.2 us
  transfers between devices with their start and end apart: 19, of which 7 were waited for; matrix products, arithmetic and copies ran while one was open for 20% of the time, Pallas kernels for 0%

profile of v1, /device:TPU:0, one launch (start us, length us, event | category | flops | bytes accessed | tf_op | source)
XLA Modules:
  0.0 477.8 jit_solution(17753981096982295856)
XLA Ops:
  9.2 1.3 dynamic_slice.3
  13.7 47.6 %all-gather.9.cloned.1.call-done = bf16[16,256,256]{2,1,0:T(8,128)(2,1)} async-done(((bf16[2,256,256]{2,1,0:T(8,128)(2,1)}), bf16[16,256,256]{2,1,0:T(8,128)(2,1)}) %all-gather.9.cloned.1.call-update) | async-done | bytes 2097168 | tf_op jit(solution)/shard_map/all_gather | solution.py:144
  61.3 1.3 slice.44
  62.6 33.3 %all-gather.5.cloned.1.call-done = bf16[1024,2048]{1,0:T(8,128)(2,1)} async-done(((bf16[1024,512]{1,0:T(8,128)(2,1)}), bf16[1024,2048]{1,0:T(8,128)(2,1)}) %all-gather.5.cloned.1.call-update) | async-done | bytes 4194320 | tf_op jit(solution)/shard_map/all_gather | solution.py:94
  95.9 3.2 fusion.1
  99.3 1.3 fusion.16
  101.7 2.0 fusion.19
  104.1 2.2 dynamic_update_slice.75
  106.4 1.1 fusion.30
  108.6 1.1 fusion.34
  113.0 1.1 fusion.42
  114.2 1.6 convert_element_type.182
  116.8 1.3 pad_maximum_fusion
  118.1 1.5 collective-permute-start.1
  119.6 1.5 collective-permute-start
  121.1 2.4 collective-permute-start.3
  123.5 1.3 copy.37
  124.8 34.0 %reduce-scatter.3.cloned.1.call-done = bf16[2,1024,256]{2,1,0:T(8,128)(2,1)} async-done(((bf16[8,1024,256]{2,1,0:T(8,128)(2,1)}), bf16[2,1024,256]{2,1,0:T(8,128)(2,1)}) %reduce-scatter.3.cloned.1.call-update) | async-done | bytes 1048592 | tf_op jit(solution)/shard_map/reduce_scatter | solution.py:111
  158.8 2.7 convert_bitcast_fusion
  161.5 1.9 copy.41
  163.5 2.7 fusion.12
  166.2 3.4 collective-permute-start.5
  169.6 2.4 multiply_convert_fusion
  172.1 1.5 collective-permute-start.2
  173.6 6.1 %broadcast_in_dim.105 = bf16[8,256,3072]{2,1,0:T(8,128)(2,1)} broadcast(bf16[]{:T(256)} %constant.163.clone.1), dimensions={} | broadcast | bytes 12582914 | tf_op jit(solution)/shard_map/broadcast_in_dim | solution.py:82
  179.7 1.4 bitcast_dynamic-update-slice_fusion.7
  181.1 53.4 %collective-permute-start.10 = (bf16[1536,256]{1,0:T(8,128)(2,1)}, bf16[1536,256]{1,0:T(8,128)(2,1)}, u32[]{:S(2)}, u32[]{:S(2)}) collective-permute-start(bf16[1536,256]{1,0:T(8,128)(2,1)} %multiply_convert_fusion), channel_id=1, source_target_pairs={{0,16},{4,20},{8,24},{12,28},{16,0},{20,4},{24,8},{28,12},{1,17},{... | collective-permute-start | bytes 2359304 | tf_op jit(solution)/shard_map/ppermute | solution.py:63
  235.0 2.7 bitcast_dynamic-update-slice_fusion.6
  237.7 2.6 bitcast_dynamic-update-slice_fusion.5
  240.3 12.6 %collective-permute-done.5 = bf16[256,3072]{1,0:T(8,128)(2,1)S(1)} collective-permute-done((bf16[256,3072]{1,0:T(8,128)(2,1)}, bf16[256,3072]{1,0:T(8,128)(2,1)S(1)}, u32[]{:S(2)}, u32[]{:S(2)}) %collective-permute-start.5) | collective-permute-done | bytes 1572896 | tf_op jit(solution)/shard_map/ppermute | solution.py:63
  252.9 30.9 %collective-permute-start.12 = (bf16[1536,256]{1,0:T(8,128)(2,1)}, bf16[1536,256]{1,0:T(8,128)(2,1)}, u32[]{:S(2)}, u32[]{:S(2)}) collective-permute-start(bf16[1536,256]{1,0:T(8,128)(2,1)} %multiply_convert_fusion), channel_id=1, source_target_pairs={{0,24},{4,28},{8,0},{12,4},{16,8},{20,12},{24,16},{28,20},{1,25},{... | collective-permute-start | bytes 2359304 | tf_op jit(solution)/shard_map/ppermute | solution.py:63
  284.4 2.7 bitcast_dynamic-update-slice_fusion.4
  287.1 2.7 bitcast_dynamic-update-slice_fusion.3
  289.8 1.5 collective-permute-start.7
  291.3 17.4 %collective-permute-done.10 = bf16[1536,256]{1,0:T(8,128)(2,1)} collective-permute-done((bf16[1536,256]{1,0:T(8,128)(2,1)}, bf16[1536,256]{1,0:T(8,128)(2,1)}, u32[]{:S(2)}, u32[]{:S(2)}) %collective-permute-start.10) | collective-permute-done | bytes 786464 | tf_op jit(solution)/shard_map/ppermute | solution.py:63
  308.6 1.5 collective-permute-start.9
  310.1 15.2 %collective-permute-done.12 = bf16[1536,256]{1,0:T(8,128)(2,1)} collective-permute-done((bf16[1536,256]{1,0:T(8,128)(2,1)}, bf16[1536,256]{1,0:T(8,128)(2,1)}, u32[]{:S(2)}, u32[]{:S(2)}) %collective-permute-start.12) | collective-permute-done | bytes 786464 | tf_op jit(solution)/shard_map/ppermute | solution.py:63
  325.4 1.5 collective-permute-start.11
  327.4 1.3 bitcast_dynamic-update-slice_fusion.2
  328.7 1.2 bitcast_dynamic-update-slice_fusion.1
  329.9 1.3 bitcast_dynamic-update-slice_fusion
  331.2 3.3 fusion.3
  334.7 17.0 %convolution_multiply_fusion = f32[1024,3072]{1,0:T(8,128)S(1)} fusion(bf16[2048,3072]{1,0:T(8,128)(2,1)} %bitcast.151, f32[1024]{0:T(1024)S(1)} %add_rsqrt_fusion, bf16[1024,2048]{0,1:T(8,128)(2,1)S(1)} %copy-done.3, f32[2048]{0:T(1024)S(1)} %copy-done.19), kind=kOutput, calls=%fused_computation.8 | convolution fusion | flops 12894339072 | bytes 29372416 | tf_op jit(solution)/shard_map/dot_general | solution.py:99
  351.7 2.2 fusion.5
  353.9 2.9 fusion.20
  356.8 2.9 fusion.22
  359.7 2.9 fusion.24
  362.6 2.9 fusion.21
  365.5 2.9 fusion.23
  368.4 2.0 copy.42
  370.5 2.1 copy.43
  372.5 2.0 copy.44
  374.6 2.0 copy.45
  376.6 2.1 copy.46
  378.7 2.9 fusion.25
  381.6 2.0 copy.47
  383.6 2.9 fusion.26
  386.5 2.0 copy.48
  388.5 2.9 fusion.27
  391.5 1.4 copy.49
  392.9 2.5 broadcast.134
  402.1 66.2 %reduce-scatter.5.cloned.1.call-done = bf16[2,1024,256]{1,2,0:T(8,128)(2,1)} async-done(((bf16[8,1024,256]{1,2,0:T(8,128)(2,1)}), bf16[2,1024,256]{1,2,0:T(8,128)(2,1)}) %reduce-scatter.5.cloned.1.call-update) | async-done | bytes 1048592 | tf_op jit(solution)/shard_map/reduce_scatter | solution.py:111
  468.3 1.6 fusion.11
  469.9 1.3 copy.50
  (92 shorter events, 18.3 us)
Async XLA Ops:
  6.5 54.8 %all-gather.9.cloned.1.call-start = ((), (), s32[]{:S(2)}) async-start(), calls=%async_computation.6 | async-start | bytes 2359296 | tf_op jit(solution)/shard_map/all_gather | solution.py:144
  7.6 91.5 %copy-start.18 = (f32[2048]{0:T(1024)S(1)}, f32[2048]{0:T(1024)}, u32[]{:S(2)}) copy-start(f32[2048]{0:T(1024)} %param.15) | copy-start | bytes 24580
  7.6 91.5 %copy-start.20 = (f32[256]{0:T(256)S(1)}, f32[256]{0:T(256)}, u32[]{:S(2)}) copy-start(f32[256]{0:T(256)} %param.17) | copy-start | bytes 3076
  8.4 87.5 %all-gather.5.cloned.1.call-start = ((), (), s32[]{:S(2)}) async-start(), calls=%async_computation.2 | async-start | bytes 5242880 | tf_op jit(solution)/shard_map/all_gather | solution.py:94
  9.1 149.7 %reduce-scatter.3.cloned.1.call-start = ((), (), s32[]{:S(2)}) async-start(), calls=%async_computation.3 | async-start | bytes 5242880 | tf_op jit(solution)/shard_map/reduce_scatter | solution.py:111
  95.9 3.4 copy-start.4
  100.6 3.2 copy-start.6
  109.7 4.4 copy-start.14
  114.1 9.4 %copy-start.5 = (bf16[1024,512]{1,0:T(8,128)(2,1)S(1)}, bf16[1024,512]{1,0:T(8,128)(2,1)}, u32[]{:S(2)}) copy-start(bf16[1024,512]{1,0:T(8,128)(2,1)} %param.14) | copy-start | bytes 3145732
  114.1 217.2 %all-gather.7.cloned.1.call-start = ((), (), s32[]{:S(2)}) async-start(), calls=%async_computation.4 | async-start | bytes 5242880 | tf_op jit(solution)/shard_map/all_gather | solution.py:94
  115.8 0.9 copy-start.1
  118.1 54.0 %collective-permute-start.1 = (bf16[256,3072]{1,0:T(8,128)(2,1)}, bf16[256,3072]{1,0:T(8,128)(2,1)}, u32[]{:S(2)}, u32[]{:S(2)}) collective-permute-start(bf16[256,3072]{1,0:T(8,128)(2,1)} %pad_maximum_fusion), channel_id=1, source_target_pairs={{0,8},{4,12},{8,16},{12,20},{16,24},{20,28},{24,0},{28,4},{1,9},{5... | collective-permute-start | bytes 4718600 | tf_op jit(solution)/shard_map/ppermute | solution.py:63
  119.6 61.5 %collective-permute-start = (bf16[256,3072]{1,0:T(8,128)(2,1)}, bf16[256,3072]{1,0:T(8,128)(2,1)}, u32[]{:S(2)}, u32[]{:S(2)}) collective-permute-start(bf16[256,3072]{1,0:T(8,128)(2,1)} %pad_maximum_fusion), channel_id=1, source_target_pairs={{0,4},{4,0},{8,12},{12,8},{16,20},{20,16},{24,28},{28,24},{1,5},{5... | collective-permute-start | bytes 4718600 | tf_op jit(solution)/shard_map/ppermute | solution.py:72
  121.1 113.4 %collective-permute-start.3 = (bf16[256,3072]{1,0:T(8,128)(2,1)}, bf16[256,3072]{1,0:T(8,128)(2,1)}, u32[]{:S(2)}, u32[]{:S(2)}) collective-permute-start(bf16[256,3072]{1,0:T(8,128)(2,1)} %pad_maximum_fusion), channel_id=1, source_target_pairs={{0,16},{4,20},{8,24},{12,28},{16,0},{20,4},{24,8},{28,12},{1,17},{... | collective-permute-start | bytes 4718600 | tf_op jit(solution)/shard_map/ppermute | solution.py:63
  161.5 8.1 %copy-start.17 = (f32[256]{0:T(256)S(1)}, f32[256]{0:T(256)}, u32[]{:S(2)}) copy-start(f32[256]{0:T(256)} %param.26) | copy-start | bytes 3076
  166.2 302.1 %reduce-scatter.5.cloned.1.call-start = ((), (), s32[]{:S(2)}) async-start(), calls=%async_computation.5 | async-start | bytes 5242880 | tf_op jit(solution)/shard_map/reduce_scatter | solution.py:111
  166.2 86.7 %collective-permute-start.5 = (bf16[256,3072]{1,0:T(8,128)(2,1)}, bf16[256,3072]{1,0:T(8,128)(2,1)S(1)}, u32[]{:S(2)}, u32[]{:S(2)}) collective-permute-start(bf16[256,3072]{1,0:T(8,128)(2,1)} %pad_maximum_fusion), channel_id=1, source_target_pairs={{0,24},{4,28},{8,0},{12,4},{16,8},{20,12},{24,16},{28,20},{1,25},{... | collective-permute-start | bytes 4718600 | tf_op jit(solution)/shard_map/ppermute | solution.py:63
  172.1 117.7 %collective-permute-start.8 = (bf16[1536,256]{1,0:T(8,128)(2,1)}, bf16[1536,256]{1,0:T(8,128)(2,1)}, u32[]{:S(2)}, u32[]{:S(2)}) collective-permute-start(bf16[1536,256]{1,0:T(8,128)(2,1)} %multiply_convert_fusion), channel_id=1, source_target_pairs={{0,8},{4,12},{8,16},{12,20},{16,24},{20,28},{24,0},{28,4},{1,9},{5... | collective-permute-start | bytes 2359304 | tf_op jit(solution)/shard_map/ppermute | solution.py:63
  172.1 7.6 %copy-start.2 = (bf16[256,1536]{1,0:T(8,128)(2,1)S(1)}, bf16[256,1536]{1,0:T(8,128)(2,1)}, u32[]{:S(2)}) copy-start(bf16[256,1536]{1,0:T(8,128)(2,1)} %copy-done.1) | copy-start | bytes 2359300
  172.1 111.8 %collective-permute-start.2 = (bf16[256,3072]{1,0:T(8,128)(2,1)}, bf16[256,3072]{1,0:T(8,128)(2,1)}, u32[]{:S(2)}, u32[]{:S(2)}) collective-permute-start(bf16[256,3072]{1,0:T(8,128)(2,1)} %collective-permute-done.1), channel_id=1, source_target_pairs={{0,4},{4,0},{8,12},{12,8},{16,20},{20,16},{24,28},{28,24},{1,5},{5... | collective-permute-start | bytes 4718600 | tf_op jit(solution)/shard_map/ppermute | solution.py:72
  181.1 127.5 %collective-permute-start.10 = (bf16[1536,256]{1,0:T(8,128)(2,1)}, bf16[1536,256]{1,0:T(8,128)(2,1)}, u32[]{:S(2)}, u32[]{:S(2)}) collective-permute-start(bf16[1536,256]{1,0:T(8,128)(2,1)} %multiply_convert_fusion), channel_id=1, source_target_pairs={{0,16},{4,20},{8,24},{12,28},{16,0},{20,4},{24,8},{28,12},{1,17},{... | collective-permute-start | bytes 2359304 | tf_op jit(solution)/shard_map/ppermute | solution.py:63
  234.5 92.3 %collective-permute-start.4 = (bf16[256,3072]{1,0:T(8,128)(2,1)}, bf16[256,3072]{1,0:T(8,128)(2,1)S(1)}, u32[]{:S(2)}, u32[]{:S(2)}) collective-permute-start(bf16[256,3072]{1,0:T(8,128)(2,1)} %collective-permute-done.3), channel_id=1, source_target_pairs={{0,4},{4,0},{8,12},{12,8},{16,20},{20,16},{24,28},{28,24},{1,5},{5... | collective-permute-start | bytes 4718600 | tf_op jit(solution)/shard_map/ppermute | solution.py:72
  252.9 72.4 %collective-permute-start.12 = (bf16[1536,256]{1,0:T(8,128)(2,1)}, bf16[1536,256]{1,0:T(8,128)(2,1)}, u32[]{:S(2)}, u32[]{:S(2)}) collective-permute-start(bf16[1536,256]{1,0:T(8,128)(2,1)} %multiply_convert_fusion), channel_id=1, source_target_pairs={{0,24},{4,28},{8,0},{12,4},{16,8},{20,12},{24,16},{28,20},{1,25},{... | collective-permute-start | bytes 2359304 | tf_op jit(solution)/shard_map/ppermute | solution.py:63
  283.9 46.1 %collective-permute-start.6 = (bf16[256,3072]{1,0:T(8,128)(2,1)S(1)}, bf16[256,3072]{1,0:T(8,128)(2,1)S(1)}, u32[]{:S(2)}, u32[]{:S(2)}) collective-permute-start(bf16[256,3072]{1,0:T(8,128)(2,1)S(1)} %collective-permute-done.5), channel_id=1, source_target_pairs={{0,4},{4,0},{8,12},{12,8},{16,20},{20,16},{24,28},{28,24},{1,5},{5... | collective-permute-start | bytes 4718600 | tf_op jit(solution)/shard_map/ppermute | solution.py:72
  289.8 72.9 %collective-permute-start.7 = (bf16[1536,256]{1,0:T(8,128)(2,1)}, bf16[1536,256]{1,0:T(8,128)(2,1)}, u32[]{:S(2)}, u32[]{:S(2)}) collective-permute-start(bf16[1536,256]{1,0:T(8,128)(2,1)} %multiply_convert_fusion), channel_id=1, source_target_pairs={{0,4},{4,0},{8,12},{12,8},{16,20},{20,16},{24,28},{28,24},{1,5},{5... | collective-permute-start | bytes 2359304 | tf_op jit(solution)/shard_map/ppermute | solution.py:72
  308.6 56.9 %collective-permute-start.9 = (bf16[1536,256]{1,0:T(8,128)(2,1)}, bf16[1536,256]{1,0:T(8,128)(2,1)}, u32[]{:S(2)}, u32[]{:S(2)}) collective-permute-start(bf16[1536,256]{1,0:T(8,128)(2,1)} %collective-permute-done.8), channel_id=1, source_target_pairs={{0,4},{4,0},{8,12},{12,8},{16,20},{20,16},{24,28},{28,24},{1,5},{5... | collective-permute-start | bytes 2359304 | tf_op jit(solution)/shard_map/ppermute | solution.py:72
  325.4 53.3 %collective-permute-start.11 = (bf16[1536,256]{1,0:T(8,128)(2,1)}, bf16[1536,256]{1,0:T(8,128)(2,1)}, u32[]{:S(2)}, u32[]{:S(2)}) collective-permute-start(bf16[1536,256]{1,0:T(8,128)(2,1)} %collective-permute-done.10), channel_id=1, source_target_pairs={{0,4},{4,0},{8,12},{12,8},{16,20},{20,16},{24,28},{28,24},{1,5},{5... | collective-permute-start | bytes 2359304 | tf_op jit(solution)/shard_map/ppermute | solution.py:72
  326.8 61.7 %collective-permute-start.13 = (bf16[1536,256]{1,0:T(8,128)(2,1)}, bf16[1536,256]{1,0:T(8,128)(2,1)}, u32[]{:S(2)}, u32[]{:S(2)}) collective-permute-start(bf16[1536,256]{1,0:T(8,128)(2,1)} %collective-permute-done.12), channel_id=1, source_target_pairs={{0,4},{4,0},{8,12},{12,8},{16,20},{20,16},{24,28},{28,24},{1,5},{5... | collective-permute-start | bytes 2359304 | tf_op jit(solution)/shard_map/ppermute | solution.py:72
  329.9 4.6 copy-start.19
  331.2 3.4 copy-start.3
  334.7 17.0 %copy-start.15 = (f32[1536]{0:T(1024)S(1)}, f32[1536]{0:T(1024)}, u32[]{:S(2)}) copy-start(f32[1536]{0:T(1024)} %param.24) | copy-start | bytes 18436
  334.7 17.0 %copy-start.16 = (f32[1536]{0:T(1024)S(1)}, f32[1536]{0:T(1024)}, u32[]{:S(2)}) copy-start(f32[1536]{0:T(1024)} %param.22) | copy-start | bytes 18436
  391.4 3.9 copy-start.13
  391.4 4.8 copy-start.12
  391.4 5.6 %copy-start.10 = (bf16[1,1024,256]{1,2,0:T(8,128)(2,1)S(1)}, bf16[1,1024,256]{1,2,0:T(8,128)(2,1)}, u32[]{:S(2)}) copy-start(bf16[1,1024,256]{1,2,0:T(8,128)(2,1)} %copy.44) | copy-start | bytes 1572868
  391.4 6.4 %copy-start.8 = (bf16[1,1024,256]{1,2,0:T(8,128)(2,1)S(1)}, bf16[1,1024,256]{1,2,0:T(8,128)(2,1)}, u32[]{:S(2)}) copy-start(bf16[1,1024,256]{1,2,0:T(8,128)(2,1)} %copy.45) | copy-start | bytes 1572868
  392.9 5.9 %copy-start.7 = (bf16[1,1024,256]{1,2,0:T(8,128)(2,1)S(1)}, bf16[1,1024,256]{1,2,0:T(8,128)(2,1)}, u32[]{:S(2)}) copy-start(bf16[1,1024,256]{1,2,0:T(8,128)(2,1)} %copy.46) | copy-start | bytes 1572868
  392.9 6.7 %copy-start.11 = (bf16[1,1024,256]{1,2,0:T(8,128)(2,1)S(1)}, bf16[1,1024,256]{1,2,0:T(8,128)(2,1)}, u32[]{:S(2)}) copy-start(bf16[1,1024,256]{1,2,0:T(8,128)(2,1)} %copy.47) | copy-start | bytes 1572868
  395.4 5.0 %copy-start.9 = (bf16[1,1024,256]{1,2,0:T(8,128)(2,1)S(1)}, bf16[1,1024,256]{1,2,0:T(8,128)(2,1)}, u32[]{:S(2)}) copy-start(bf16[1,1024,256]{1,2,0:T(8,128)(2,1)} %copy.48) | copy-start | bytes 1572868
  398.7 69.6 %copy-start = (bf16[1024,512]{0,1:T(8,128)(2,1)S(1)}, bf16[1024,512]{0,1:T(8,128)(2,1)}, u32[]{:S(2)}) copy-start(bf16[1024,512]{0,1:T(8,128)(2,1)} %fusion.12) | copy-start | bytes 3145732
Sparse Core Ops, SparseCore 0:
  9.5 51.7 all-gather.8
  62.9 32.9 all-gather.4
  114.2 44.5 reduce-scatter.2
  166.3 34.4 all-gather.6
  402.2 66.0 reduce-scatter.4
